TPU v7x, 32 devices: a whole 2x2x4 slice. The times are simulated.
32 devices in a mesh: fs: 16 (over z, y, core), tp: 2 (over x).
Axes of the slice: x: 2, y: 2, z: 4, core: 2. Of those that a mesh axis runs over, the one named last changes fastest.
Arguments:
- inputs: bfloat16 [32768, 2048], P('fs'), may hold values from -6 to 6
- key_grads: bfloat16 [32768, 1024], P('fs', 'tp'), may hold values from -0.078125 to 0.078125
- weights: float32 [2048, 1024], P('fs', 'tp'), may hold values from -6 to 6
- momentum: float32 [2048, 1024], P('fs', 'tp'), may hold values from -6 to 6
- left_stat: float32 [4, 2048, 2048], P('tp', 'fs'), may hold values from -96 to 96
- right_stat: float32 [8, 128, 128], P('tp'), may hold values from -256 to 256
- left_root: bfloat16 [4, 2048, 2048], P('tp', 'fs'), may hold values from -0.125 to 0.125
- right_root: bfloat16 [8, 128, 128], P('tp'), may hold values from -0.5 to 0.5
Outputs:
- momentum_next: float32 [2048, 1024], P('fs', 'tp')
- left_next: float32 [4, 2048, 2048], P('tp', 'fs')
- right_next: float32 [8, 128, 128], P('tp')
- update: float32 [2048, 1024], P('fs', 'tp')
- weights_next: float32 [2048, 1024], P('fs', 'tp')
- weights_copy: bfloat16 [2048, 1024], P(None, 'tp')
All inputs are finite; a program needn't handle non-finite values.
Results may differ from a plain program's by a relative error of at most 0.0033.
Values may be sent and summed in bfloat16 or wider, within the bound.
A program may use at most 64 MiB of HBM per device.

v0:
```python
import jax
import jax.numpy as jnp
from jax import lax
from jax.sharding import PartitionSpec as P


def body(inputs, key_grads, weights, momentum, left_stat, right_stat, left_root, right_root):
    row_count = weights.shape[0]
    col_count = weights.shape[1]
    block_count = left_root.shape[0]
    head_count = right_root.shape[0]
    head_size = right_root.shape[1]
    model_width = inputs.shape[1]
    partial_grad = lax.dot_general(
        inputs, key_grads, (((0,), (0,)), ((), ())), preferred_element_type=jnp.float32
    )
    summed = lax.psum(partial_grad, "fs")
    whole_bf = summed.astype(jnp.bfloat16)
    row_offset = lax.axis_index("fs") * row_count
    grad = lax.dynamic_slice_in_dim(summed, row_offset, row_count, 0)
    own_rows = lax.dynamic_slice_in_dim(whole_bf, row_offset, row_count, 0)
    whole_blocks = whole_bf.reshape(model_width, block_count, -1)
    left_part = jnp.einsum(
        "brd,dbc->rbc", left_root, whole_blocks, preferred_element_type=jnp.float32
    ).reshape(row_count, col_count)
    row_gram = jnp.einsum(
        "rbc,dbc->brd",
        own_rows.reshape(row_count, block_count, -1),
        whole_blocks,
        preferred_element_type=jnp.float32,
    )
    whole_heads = whole_bf.reshape(model_width, head_count, head_size)
    head_gram = jnp.einsum(
        "dhi,dhj->hij", whole_heads, whole_heads, preferred_element_type=jnp.float32
    )
    left_bf = left_part.astype(jnp.bfloat16)
    precond = jnp.einsum(
        "rhi,hij->rhj",
        left_bf.reshape(row_count, head_count, head_size),
        right_root,
        preferred_element_type=jnp.float32,
    ).reshape(row_count, col_count)
    left_next = 0.95 * left_stat + 0.05 * row_gram
    right_next = 0.95 * right_stat + 0.05 * head_gram
    grad_square, precond_square = lax.psum(
        (jnp.sum(grad * grad), jnp.sum(precond * precond)), ("fs", "tp")
    )
    scale = jnp.sqrt(grad_square / (precond_square + 1e-06))
    momentum_next = 0.9 * momentum + scale * precond
    update = -0.25 * (momentum_next + 0.4 * weights)
    weights_next = weights + update
    weights_copy = lax.all_gather(weights_next.astype(jnp.bfloat16), "fs", axis=0, tiled=True)
    return (momentum_next, left_next, right_next, update, weights_next, weights_copy)


def solution(mesh):
    in_specs = (
        P("fs", None),
        P("fs", "tp"),
        P("fs", "tp"),
        P("fs", "tp"),
        P("tp", "fs", None),
        P("tp", None, None),
        P("tp", "fs", None),
        P("tp", None, None),
    )
    out_specs = (
        P("fs", "tp"),
        P("tp", "fs", None),
        P("tp", None, None),
        P("fs", "tp"),
        P("fs", "tp"),
        P(None, "tp"),
    )
    return jax.shard_map(body, mesh=mesh, in_specs=in_specs, out_specs=out_specs, check_vma=False)
```

profile of v0, /device:TPU:0, one launch (start us, length us, event | category | flops | bytes accessed | tf_op | source)
XLA Modules:
  0.0 232.3 jit_solution(892505422793026913)
XLA Ops:
  7.2 0.0 copy-start
  7.2 0.0 all-reduce.3.cloned.1.call-start
  7.2 1.5 copy-done
  8.8 9.8 %fusion.19 = f32[2048,512]{1,0:T(8,128)} fusion(bf16[2048,2048]{1,0:T(8,128)(2,1)} %param.8, bf16[2048,512]{1,0:T(8,128)(2,1)S(1)} %copy-done), kind=kOutput, calls=%fused_computation.20 | convolution fusion | flops 4294967296 | bytes 14680064 | tf_op jit(solution)/shard_map/dot_general | solution.py:14
  18.6 0.0 all-reduce.3.cloned.1.call-update
  18.6 0.0 all-gather.2.cloned.1.call-start
  18.6 113.9 %all-reduce.3.cloned.1.call-done = f32[2048,512]{1,0:T(8,128)} async-done(((f32[2048,512]{1,0:T(8,128)}), f32[2048,512]{1,0:T(8,128)}) %all-reduce.3.cloned.1.call-update) | async-done | bytes 4194320 | tf_op jit(solution)/shard_map/psum | solution.py:17
  132.6 0.0 copy-start.8
  132.6 2.5 %convert_element_type.16 = bf16[2048,512]{1,0:T(8,128)(2,1)S(1)} convert(f32[2048,512]{1,0:T(8,128)} %all-reduce.3.cloned.1.call-done) | non-fusion elementwise | flops 1048576 | bytes 6291456 | tf_op jit(solution)/shard_map/convert_element_type | solution.py:18
  135.1 0.0 copy-start.1
  135.1 0.0 copy-start.7
  135.2 0.0 copy-done.8
  135.2 0.0 copy-start.5
  135.2 0.0 copy-start.6
  135.2 0.9 fusion.15
  136.1 0.1 copy-done.7
  136.2 0.0 copy-start.4
  136.2 0.9 multiply_reduce_fusion
  137.1 0.0 copy-done.1
  137.1 1.6 multiply_reduce_fusion.1
  138.7 39.7 %all-reduce = (f32[]{:T(128)}, f32[]{:T(128)}) all-reduce(f32[]{:T(128)} %multiply_reduce_fusion.1, f32[]{:T(128)} %get-tuple-element.12), channel_id=1, replica_groups=mesh['fs'=16,'tp'=2] {'fs','tp'}, use_global_device_ids=true, to_apply=%region_2.0 | all-reduce | flops 2 | bytes 16 | tf_op jit(solution)/shard_map/psum | solution.py:45
  179.8 0.1 copy.24
  179.9 0.0 copy-done.5
  179.9 0.0 copy-done.6
  179.9 1.0 fusion.18
  181.0 0.0 all-gather.2.cloned.1.call-update
  181.0 0.9 constant_dynamic-slice_fusion
  181.9 0.1 copy.25
  182.0 0.0 copy-done.4
  182.0 0.0 copy-start.2
  182.1 0.0 copy-start.3
  182.1 5.6 %fusion.12 = f32[4,128,128]{2,1,0:T(8,128)} fusion(f32[4,128,128]{2,1,0:T(8,128)S(1)} %copy-done.4, f32[2048,512]{1,0:T(8,128)} %all-reduce.3.cloned.1.call-done), kind=kOutput, calls=%fused_computation.11 | convolution fusion | flops 269680640 | bytes 4718592 | tf_op jit(solution)/shard_map/dhi,dhj->hij/dot_general | solution.py:33
  187.7 0.0 copy-done.2
  187.7 0.0 copy-done.3
  187.7 2.2 fusion
  189.9 32.6 %all-gather.2.cloned.1.call-done = bf16[2048,512]{1,0:T(8,128)(2,1)} async-done(((bf16[128,512]{1,0:T(8,128)(2,1)}), bf16[2048,512]{1,0:T(8,128)(2,1)}) %all-gather.2.cloned.1.call-update) | async-done | bytes 2097168 | tf_op jit(solution)/shard_map/all_gather | solution.py:52
  222.4 3.0 %copy.55 = bf16[2048,512]{1,0:T(8,128)(2,1)} copy(bf16[2048,512]{1,0:T(8,128)(2,1)} %all-gather.2.cloned.1.call-done) | data formatting | bytes 4194304
  (1 shorter events, 0.0 us)
Async XLA Ops:
  7.2 1.6 copy-start
  7.2 125.4 %all-reduce.3.cloned.1.call-start = ((), (), s32[]{:S(2)}) async-start(), calls=%async_computation | async-start | bytes 8388608 | tf_op jit(solution)/shard_map/psum | solution.py:17
  18.6 203.8 %all-gather.2.cloned.1.call-start = ((), (), s32[]{:S(2)}) async-start(), calls=%async_computation.1 | async-start | bytes 2228224 | tf_op jit(solution)/shard_map/all_gather | solution.py:52
  132.6 2.6 %copy-start.8 = (bf16[2,128,2048]{2,1,0:T(8,128)(2,1)S(1)}, bf16[2,128,2048]{2,1,0:T(8,128)(2,1)}, u32[]{:S(2)}) copy-start(bf16[2,128,2048]{2,1,0:T(8,128)(2,1)} %param.14) | copy-start | bytes 3145732
  135.1 1.9 copy-start.1
  135.1 1.0 copy-start.7
  135.2 44.7 %copy-start.5 = (f32[128,512]{1,0:T(8,128)S(1)}, f32[128,512]{1,0:T(8,128)}, u32[]{:S(2)}) copy-start(f32[128,512]{1,0:T(8,128)} %param.10) | copy-start | bytes 786436
  135.2 44.7 %copy-start.6 = (f32[128,512]{1,0:T(8,128)S(1)}, f32[128,512]{1,0:T(8,128)}, u32[]{:S(2)}) copy-start(f32[128,512]{1,0:T(8,128)} %param.11) | copy-start | bytes 786436
  136.2 45.8 %copy-start.4 = (f32[4,128,128]{2,1,0:T(8,128)S(1)}, f32[4,128,128]{2,1,0:T(8,128)}, u32[]{:S(2)}) copy-start(f32[4,128,128]{2,1,0:T(8,128)} %param.13) | copy-start | bytes 786436
  182.0 5.6 %copy-start.2 = (bf16[2048,512]{1,0:T(8,128)(2,1)S(1)}, bf16[2048,512]{1,0:T(8,128)(2,1)}, u32[]{:S(2)}) copy-start(bf16[2048,512]{1,0:T(8,128)(2,1)} %copy-done.1) | copy-start | bytes 6291460
  182.1 5.6 %copy-start.3 = (f32[2,128,2048]{2,1,0:T(8,128)S(1)}, f32[2,128,2048]{2,1,0:T(8,128)}, u32[]{:S(2)}) copy-start(f32[2,128,2048]{2,1,0:T(8,128)} %param.12) | copy-start | bytes 6291460
Sparse Core Ops, SparseCore 0:
  18.7 113.8 all-reduce.2
  181.1 41.2 all-gather.1
where the time goes:
time: 233 us; the launch traced here: 232 us
  waiting for transfers between devices  147 us (63%)
  blocking collectives  39.7 us (17%)
  matrix products  19.4 us (8%)
  between operations  15.5 us (7%)
  local copies, waits for them, and re-layouts  5.87 us (3%)
  other arithmetic  5.21 us (2%)
    psum x1, waiting for transfers between devices, body(): summed = lax.psum(partial_grad, 'fs')  114 us
    psum x1, blocking collectives, body(): lax.psum((jnp.sum(grad * grad), jnp.sum(precond * precond)), ('fs', 'tp'))  39.7 us
    all_gather x1, waiting for transfers between devices, body(): lax.all_gather(weights_next.astype(jnp.bfloat16), 'fs', axis=0, tiled=True)  32.6 us
    dot_general x1, matrix products, body(): lax.dot_general(inputs, key_grads, (((0,), (0,)), ((), ())), preferred_el...  9.81 us
    dot_general x1, matrix products, body(): jnp.einsum('dhi,dhj->hij', whole_heads, whole_heads, preferred_element_ty...  5.61 us
    unnamed x19, local copies, waits for them, and re-layouts  4.7 us
  transfers between devices with their start and end apart: 2, of which 2 were waited for; matrix products, arithmetic and copies ran while one was open for 4% of the time, Pallas kernels for 0%

commit v1 on v0

--- a/solution.py
+++ b/solution.py
@@ -14,7 +14,9 @@
     partial_grad = lax.dot_general(
         inputs, key_grads, (((0,), (0,)), ((), ())), preferred_element_type=jnp.float32
     )
-    summed = lax.psum(partial_grad, "fs")
+    summed = partial_grad
+    for hop in (1, 2, 4, 8):
+        summed = summed + lax.ppermute(summed, "fs", [(dev, dev ^ hop) for dev in range(16)])
     whole_bf = summed.astype(jnp.bfloat16)
     row_offset = lax.axis_index("fs") * row_count
     grad = lax.dynamic_slice_in_dim(summed, row_offset, row_count, 0)

time: 233 us -> 498 us (2.14)
  waiting for transfers between devices: 147 us -> 403 us
  starting transfers between devices: 0.08 us -> 7.93 us
  other arithmetic: 5.21 us -> 11.5 us
  matrix products: 19.4 us -> 14.3 us
    ppermute x0 -> x4, waiting for transfers between devices: none -> 368 us  [body(): lax.ppermute(summed, 'fs', [(dev, dev ^ hop) for dev in range(16)])]
    psum x1 -> x0, waiting for transfers between devices: 114 us -> none  [body(): summed = lax.psum(partial_grad, 'fs')]
    ppermute x0 -> x4, starting transfers between devices: none -> 7.89 us  [body(): lax.ppermute(summed, 'fs', [(dev, dev ^ hop) for dev in range(16)])]
  transfers between devices with their start and end apart: 2 -> 5, of which waited for: 2 -> 5; matrix products, arithmetic and copies ran while one was open for 4% -> 1% of each run, Pallas kernels for 0% -> 0%
where the time goes in v1:
time: 498 us
  waiting for transfers between devices  403 us (81%)
  blocking collectives  39.7 us (8%)
  between operations  15.5 us (3%)
  matrix products  14.3 us (3%)
  other arithmetic  11.5 us (2%)
  starting transfers between devices  7.93 us (2%)
  local copies, waits for them, and re-layouts  5.68 us (1%)
    ppermute x4, waiting for transfers between devices, body(): lax.ppermute(summed, 'fs', [(dev, dev ^ hop) for dev in range(16)])  368 us
    psum x1, blocking collectives, body(): lax.psum((jnp.sum(grad * grad), jnp.sum(precond * precond)), ('fs', 'tp'))  39.7 us
    all_gather x1, waiting for transfers between devices, body(): lax.all_gather(weights_next.astype(jnp.bfloat16), 'fs', axis=0, tiled=True)  35.5 us
  transfers between devices with their start and end apart: 5, of which 5 were waited for; matrix products, arithmetic and copies ran while one was open for 1% of the time, Pallas kernels for 0%

profile of v1, /device:TPU:0, one launch (start us, length us, event | category | flops | bytes accessed | tf_op | source)
XLA Modules:
  0.0 497.7 jit_solution(17114781595051486600)
XLA Ops:
  7.2 0.0 copy-start
  7.2 0.0 all-gather.2.cloned.1.call-start
  7.2 1.5 copy-done
  8.8 6.9 %fusion.4 = f32[2048,512]{0,1:T(8,128)S(1)} fusion(bf16[2048,2048]{1,0:T(8,128)(2,1)} %param.8, bf16[2048,512]{1,0:T(8,128)(2,1)S(1)} %copy-done), kind=kOutput, calls=%fused_computation.13 | convolution fusion | flops 4294967296 | bytes 14680064 | tf_op jit(solution)/shard_map/dot_general | solution.py:14
  15.7 0.6 collective-permute-start
  16.3 6.8 %collective-permute-done = f32[2048,512]{0,1:T(8,128)S(1)} collective-permute-done((f32[2048,512]{0,1:T(8,128)S(1)}, f32[2048,512]{0,1:T(8,128)S(1)}, u32[]{:S(2)}, u32[]{:S(2)}) %collective-permute-start) | collective-permute-done | bytes 4194336 | tf_op jit(solution)/shard_map/ppermute | solution.py:19
  23.1 1.1 add.38
  24.1 2.9 collective-permute-start.1
  27.1 90.9 %collective-permute-done.1 = f32[2048,512]{0,1:T(8,128)S(1)} collective-permute-done((f32[2048,512]{0,1:T(8,128)S(1)}, f32[2048,512]{0,1:T(8,128)S(1)}, u32[]{:S(2)}, u32[]{:S(2)}) %collective-permute-start.1) | collective-permute-done | bytes 4194336 | tf_op jit(solution)/shard_map/ppermute | solution.py:19
  118.0 1.1 add.39
  119.0 1.9 collective-permute-start.2
  120.9 90.2 %collective-permute-done.2 = f32[2048,512]{0,1:T(8,128)S(1)} collective-permute-done((f32[2048,512]{0,1:T(8,128)S(1)}, f32[2048,512]{0,1:T(8,128)S(1)}, u32[]{:S(2)}, u32[]{:S(2)}) %collective-permute-start.2) | collective-permute-done | bytes 4194336 | tf_op jit(solution)/shard_map/ppermute | solution.py:19
  211.1 2.7 add.40
  213.9 2.5 collective-permute-start.3
  216.4 0.0 copy-start.8
  216.4 179.7 %collective-permute-done.3 = f32[2048,512]{0,1:T(8,128)} collective-permute-done((f32[2048,512]{0,1:T(8,128)}, f32[2048,512]{0,1:T(8,128)}, u32[]{:S(2)}, u32[]{:S(2)}) %collective-permute-start.3) | collective-permute-done | bytes 4194336 | tf_op jit(solution)/shard_map/ppermute | solution.py:19
  396.1 4.9 fusion.3
  401.0 0.0 copy-start.1
  401.0 0.0 copy-start.7
  401.1 0.7 multiply_reduce_fusion.1
  401.7 0.0 copy-done.8
  401.7 0.0 copy-start.5
  401.7 0.0 copy-start.6
  401.7 0.7 convolution_convert_fusion
  402.4 0.0 copy-start.4
  402.5 0.0 copy-done.7
  402.5 0.9 multiply_reduce_fusion
  403.3 0.0 copy-done.1
  403.3 39.7 %all-reduce = (f32[]{:T(128)}, f32[]{:T(128)}) all-reduce(f32[]{:T(128)} %multiply_reduce_fusion.1, f32[]{:T(128)} %get-tuple-element.14), channel_id=1, replica_groups=mesh['fs'=16,'tp'=2] {'fs','tp'}, use_global_device_ids=true, to_apply=%region_1.0 | all-reduce | flops 2 | bytes 16 | tf_op jit(solution)/shard_map/psum | solution.py:47
  444.4 0.1 copy.21
  444.5 0.0 copy-done.5
  444.5 0.0 copy-done.6
  444.5 1.0 fusion.2
  445.5 0.0 all-gather.2.cloned.1.call-update
  445.6 0.9 constant_dynamic-slice_fusion
  446.5 0.0 copy-done.4
  446.5 0.0 copy-start.2
  446.5 0.0 copy-start.3
  446.5 3.8 fusion.1
  450.3 0.0 copy-done.2
  450.3 0.0 copy-done.3
  450.3 2.0 fusion
  452.3 35.5 %all-gather.2.cloned.1.call-done = bf16[2048,512]{1,0:T(8,128)(2,1)} async-done(((bf16[128,512]{1,0:T(8,128)(2,1)}), bf16[2048,512]{1,0:T(8,128)(2,1)}) %all-gather.2.cloned.1.call-update) | async-done | bytes 2097168 | tf_op jit(solution)/shard_map/all_gather | solution.py:54
  487.8 3.0 copy.31
  (1 shorter events, 0.0 us)
Async XLA Ops:
  7.2 1.6 copy-start
  7.2 480.6 %all-gather.2.cloned.1.call-start = ((), (), s32[]{:S(2)}) async-start(), calls=%async_computation | async-start | bytes 2228224 | tf_op jit(solution)/shard_map/all_gather | solution.py:54
  15.7 7.3 %collective-permute-start = (f32[2048,512]{0,1:T(8,128)S(1)}, f32[2048,512]{0,1:T(8,128)S(1)}, u32[]{:S(2)}, u32[]{:S(2)}) collective-permute-start(f32[2048,512]{0,1:T(8,128)S(1)} %fusion.4), channel_id=1, source_target_pairs={{0,2},{2,0},{4,6},{6,4},{8,10},{10,8},{12,14},{14,12},{16,18},{18,... | collective-permute-start | bytes 12582920 | tf_op jit(solution)/shard_map/ppermute | solution.py:19
  24.1 93.8 %collective-permute-start.1 = (f32[2048,512]{0,1:T(8,128)S(1)}, f32[2048,512]{0,1:T(8,128)S(1)}, u32[]{:S(2)}, u32[]{:S(2)}) collective-permute-start(f32[2048,512]{0,1:T(8,128)S(1)} %add.38), channel_id=1, source_target_pairs={{0,4},{2,6},{4,0},{6,2},{8,12},{10,14},{12,8},{14,10},{16,20},{18,... | collective-permute-start | bytes 12582920 | tf_op jit(solution)/shard_map/ppermute | solution.py:19
  119.0 92.1 %collective-permute-start.2 = (f32[2048,512]{0,1:T(8,128)S(1)}, f32[2048,512]{0,1:T(8,128)S(1)}, u32[]{:S(2)}, u32[]{:S(2)}) collective-permute-start(f32[2048,512]{0,1:T(8,128)S(1)} %add.39), channel_id=1, source_target_pairs={{0,8},{2,10},{4,12},{6,14},{8,0},{10,2},{12,4},{14,6},{16,24},{18,... | collective-permute-start | bytes 12582920 | tf_op jit(solution)/shard_map/ppermute | solution.py:19
  213.9 182.3 %collective-permute-start.3 = (f32[2048,512]{0,1:T(8,128)}, f32[2048,512]{0,1:T(8,128)}, u32[]{:S(2)}, u32[]{:S(2)}) collective-permute-start(f32[2048,512]{0,1:T(8,128)} %add.40), channel_id=1, source_target_pairs={{0,16},{2,18},{4,20},{6,22},{8,24},{10,26},{12,28},{14,30},{16,0},... | collective-permute-start | bytes 12582920 | tf_op jit(solution)/shard_map/ppermute | solution.py:19
  216.4 185.3 %copy-start.8 = (bf16[2,128,2048]{2,1,0:T(8,128)(2,1)S(1)}, bf16[2,128,2048]{2,1,0:T(8,128)(2,1)}, u32[]{:S(2)}) copy-start(bf16[2,128,2048]{2,1,0:T(8,128)(2,1)} %param.14) | copy-start | bytes 3145732
  401.0 2.3 copy-start.1
  401.0 1.4 copy-start.7
  401.7 42.8 %copy-start.5 = (f32[128,512]{1,0:T(8,128)S(1)}, f32[128,512]{1,0:T(8,128)}, u32[]{:S(2)}) copy-start(f32[128,512]{1,0:T(8,128)} %param.10) | copy-start | bytes 786436
  401.7 42.8 %copy-start.6 = (f32[128,512]{1,0:T(8,128)S(1)}, f32[128,512]{1,0:T(8,128)}, u32[]{:S(2)}) copy-start(f32[128,512]{1,0:T(8,128)} %param.11) | copy-start | bytes 786436
  402.4 44.0 %copy-start.4 = (f32[4,128,128]{2,1,0:T(8,128)S(1)}, f32[4,128,128]{2,1,0:T(8,128)}, u32[]{:S(2)}) copy-start(f32[4,128,128]{2,1,0:T(8,128)} %param.13) | copy-start | bytes 786436
  446.5 3.8 copy-start.2
  446.5 3.8 copy-start.3
Sparse Core Ops, SparseCore 0:
  445.7 42.0 all-gather.1

commit v2 on v0

--- a/solution.py
+++ b/solution.py
@@ -49,7 +49,12 @@
     momentum_next = 0.9 * momentum + scale * precond
     update = -0.25 * (momentum_next + 0.4 * weights)
     weights_next = weights + update
-    weights_copy = lax.all_gather(weights_next.astype(jnp.bfloat16), "fs", axis=0, tiled=True)
+    weights_copy = jnp.concatenate(
+        lax.all_to_all(
+            jnp.stack([weights_next.astype(jnp.bfloat16)] * lax.axis_size("fs")), "fs", 0, 0
+        ),
+        axis=0,
+    )
     return (momentum_next, left_next, right_next, update, weights_next, weights_copy)
 
 

time: 233 us -> 245 us (1.052)
  the two profiles are of different devices: /device:TPU:0 before, /device:TPU:13 now
where the time goes in v2:
time: 245 us
  waiting for transfers between devices  150 us (61%)
  blocking collectives  39.8 us (16%)
  matrix products  19.4 us (8%)
  between operations  15.5 us (6%)
  local copies, waits for them, and re-layouts  7.42 us (3%)
  starting transfers between devices  7.35 us (3%)
  other arithmetic  5.18 us (2%)
    psum x1, waiting for transfers between devices, body(): summed = lax.psum(partial_grad, 'fs')  111 us
    psum x1, blocking collectives, body(): lax.psum((jnp.sum(grad * grad), jnp.sum(precond * precond)), ('fs', 'tp'))  39.8 us
    all_to_all x1, waiting for transfers between devices, body(): lax.all_to_all(jnp.stack([weights_next.astype(jnp.bfloat16)] * lax.axis_s...  38.7 us
    dot_general x1, matrix products, body(): lax.dot_general(inputs, key_grads, (((0,), (0,)), ((), ())), preferred_el...  9.81 us
    all_to_all x1, starting transfers between devices, body(): lax.all_to_all(jnp.stack([weights_next.astype(jnp.bfloat16)] * lax.axis_s...  7.31 us
    dot_general x1, matrix products, body(): jnp.einsum('dhi,dhj->hij', whole_heads, whole_heads, preferred_element_ty...  5.62 us
  transfers between devices with their start and end apart: 2, of which 2 were waited for; matrix products, arithmetic and copies ran while one was open for 4% of the time, Pallas kernels for 0%

profile of v2, /device:TPU:13, one launch (start us, length us, event | category | flops | bytes accessed | tf_op | source)
XLA Modules:
  0.0 244.5 jit_solution(11632135612856630964)
XLA Ops:
  7.2 0.0 copy-start
  7.2 0.0 all-reduce.3.cloned.1.call-start
  7.2 1.5 copy-done
  8.8 9.8 %fusion.19 = f32[2048,512]{1,0:T(8,128)} fusion(bf16[2048,2048]{1,0:T(8,128)(2,1)} %param.8, bf16[2048,512]{1,0:T(8,128)(2,1)S(1)} %copy-done), kind=kOutput, calls=%fused_computation.20 | convolution fusion | flops 4294967296 | bytes 14680064 | tf_op jit(solution)/shard_map/dot_general | solution.py:14
  18.6 0.0 all-reduce.3.cloned.1.call-update
  18.6 111.2 %all-reduce.3.cloned.1.call-done = f32[2048,512]{1,0:T(8,128)} async-done(((f32[2048,512]{1,0:T(8,128)}), f32[2048,512]{1,0:T(8,128)}) %all-reduce.3.cloned.1.call-update) | async-done | bytes 4194320 | tf_op jit(solution)/shard_map/psum | solution.py:17
  129.9 0.0 copy-start.8
  129.9 2.5 %convert_element_type.16 = bf16[2048,512]{1,0:T(8,128)(2,1)S(1)} convert(f32[2048,512]{1,0:T(8,128)} %all-reduce.3.cloned.1.call-done) | non-fusion elementwise | flops 1048576 | bytes 6291456 | tf_op jit(solution)/shard_map/convert_element_type | solution.py:18
  132.4 0.0 copy-start.1
  132.4 0.0 copy-start.7
  132.4 0.0 copy-done.8
  132.4 0.0 copy-start.5
  132.4 0.0 copy-start.6
  132.5 0.9 fusion.15
  133.4 0.1 copy-done.7
  133.5 0.9 multiply_reduce_fusion
  134.3 0.0 copy-done.1
  134.3 1.6 multiply_reduce_fusion.1
  136.0 39.8 %all-reduce = (f32[]{:T(128)}, f32[]{:T(128)}) all-reduce(f32[]{:T(128)} %multiply_reduce_fusion.1, f32[]{:T(128)} %get-tuple-element.12), channel_id=1, replica_groups=mesh['fs'=16,'tp'=2] {'fs','tp'}, use_global_device_ids=true, to_apply=%region_2.0 | all-reduce | flops 2 | bytes 16 | tf_op jit(solution)/shard_map/psum | solution.py:45
  177.1 0.1 copy.24
  177.2 0.0 copy-done.5
  177.2 0.0 copy-done.6
  177.3 1.0 fusion.18
  178.3 1.6 stack.2
  179.8 0.0 copy-start.4
  179.8 7.3 %all-to-all-start = ((bf16[16,128,512]{2,1,0:T(8,128)(2,1)}), bf16[16,128,512]{2,1,0:T(8,128)(2,1)}, u32[]{:S(2)}, u32[]{:S(2)}) async-start(bf16[16,128,512]{2,1,0:T(8,128)(2,1)} %stack.2), calls=%async_computation | async-start | bytes 4194304 | tf_op jit(solution)/shard_map/all_to_all | solution.py:53
  187.1 0.9 constant_dynamic-slice_fusion
  188.0 0.1 copy.25
  188.2 0.0 copy-done.4
  188.2 0.0 copy-start.2
  188.2 0.0 copy-start.3
  188.2 5.6 %fusion.12 = f32[4,128,128]{2,1,0:T(8,128)} fusion(f32[4,128,128]{2,1,0:T(8,128)S(1)} %copy-done.4, f32[2048,512]{1,0:T(8,128)} %all-reduce.3.cloned.1.call-done), kind=kOutput, calls=%fused_computation.11 | convolution fusion | flops 269680640 | bytes 4718592 | tf_op jit(solution)/shard_map/dhi,dhj->hij/dot_general | solution.py:33
  193.8 0.0 copy-done.2
  193.8 0.0 copy-done.3
  193.8 2.2 fusion
  196.0 38.7 %all-to-all-done = bf16[16,128,512]{2,1,0:T(8,128)(2,1)} async-done(((bf16[16,128,512]{2,1,0:T(8,128)(2,1)}), bf16[16,128,512]{2,1,0:T(8,128)(2,1)}, u32[]{:S(2)}, u32[]{:S(2)}) %all-to-all-start) | async-done | bytes 2097184 | tf_op jit(solution)/shard_map/all_to_all | solution.py:53
  234.7 3.0 %copy.55 = bf16[2048,512]{1,0:T(8,128)(2,1)} copy(bf16[2048,512]{1,0:T(8,128)(2,1)} %bitcast.5) | data formatting | bytes 4194304
  (1 shorter events, 0.0 us)
Async XLA Ops:
  7.2 1.6 copy-start
  7.2 122.7 %all-reduce.3.cloned.1.call-start = ((), (), s32[]{:S(2)}) async-start(), calls=%async_computation.1 | async-start | bytes 8388608 | tf_op jit(solution)/shard_map/psum | solution.py:17
  129.9 2.6 %copy-start.8 = (bf16[2,128,2048]{2,1,0:T(8,128)(2,1)S(1)}, bf16[2,128,2048]{2,1,0:T(8,128)(2,1)}, u32[]{:S(2)}) copy-start(bf16[2,128,2048]{2,1,0:T(8,128)(2,1)} %param.14) | copy-start | bytes 3145732
  132.4 1.9 copy-start.1
  132.4 1.0 copy-start.7
  132.4 44.8 %copy-start.5 = (f32[128,512]{1,0:T(8,128)S(1)}, f32[128,512]{1,0:T(8,128)}, u32[]{:S(2)}) copy-start(f32[128,512]{1,0:T(8,128)} %param.10) | copy-start | bytes 786436
  132.4 44.8 %copy-start.6 = (f32[128,512]{1,0:T(8,128)S(1)}, f32[128,512]{1,0:T(8,128)}, u32[]{:S(2)}) copy-start(f32[128,512]{1,0:T(8,128)} %param.11) | copy-start | bytes 786436
  179.8 8.4 %copy-start.4 = (f32[4,128,128]{2,1,0:T(8,128)S(1)}, f32[4,128,128]{2,1,0:T(8,128)}, u32[]{:S(2)}) copy-start(f32[4,128,128]{2,1,0:T(8,128)} %param.13) | copy-start | bytes 786436
  179.8 54.8 %all-to-all-start = ((bf16[16,128,512]{2,1,0:T(8,128)(2,1)}), bf16[16,128,512]{2,1,0:T(8,128)(2,1)}, u32[]{:S(2)}, u32[]{:S(2)}) async-start(bf16[16,128,512]{2,1,0:T(8,128)(2,1)} %stack.2), calls=%async_computation | async-start | bytes 4194304 | tf_op jit(solution)/shard_map/all_to_all | solution.py:53
  188.2 5.6 %copy-start.2 = (bf16[2048,512]{1,0:T(8,128)(2,1)S(1)}, bf16[2048,512]{1,0:T(8,128)(2,1)}, u32[]{:S(2)}) copy-start(bf16[2048,512]{1,0:T(8,128)(2,1)} %copy-done.1) | copy-start | bytes 6291460
  188.2 5.6 %copy-start.3 = (f32[2,128,2048]{2,1,0:T(8,128)S(1)}, f32[2,128,2048]{2,1,0:T(8,128)}, u32[]{:S(2)}) copy-start(f32[2,128,2048]{2,1,0:T(8,128)} %param.12) | copy-start | bytes 6291460
Sparse Core Ops, SparseCore 0:
  18.7 111.0 all-reduce.2
